TPU v7x, 32 devices: a whole 2x2x4 slice. The times are simulated.
32 devices in a mesh: kv: 8 (over z, y), tp: 4 (over x, core).
Axes of the slice: x: 2, y: 2, z: 4, core: 2. Of those that a mesh axis runs over, the one named last changes fastest.
Arguments:
- tokens: bfloat16 [32, 4096], P(None, 'kv'), may hold values from -40 to 40, as said below
- norm_gain: float32 [4096], P('kv'), may hold values from 0.1 to 1.9
- w_query: bfloat16 [4096, 2048], P('kv', 'tp'), may hold values from -0.09375 to 0.09375
- w_key: bfloat16 [4096, 512], P('kv', 'tp'), may hold values from -0.09375 to 0.09375
- w_value: bfloat16 [4096, 512], P('kv', 'tp'), may hold values from -0.09375 to 0.09375
- forget_weight: bfloat16 [4096, 32], replicated, may hold values from -0.09375 to 0.09375
- forget_bias: float32 [32], P('tp'), may hold values from -1 to 3
- kv_cache: bfloat16 [32, 10240, 8, 128], P(None, 'kv', 'tp'), may hold values from -6 to 6
- cum_gates: float32 [32, 32, 10240], P(None, 'tp', 'kv'), may hold values from -10500 to 0, as said below
- lengths: int32 [32], replicated, may hold values from 1 to 10240, as said below
- w_out: bfloat16 [2048, 4096], P('tp', 'kv'), may hold values from -0.25 to 0.25
Outputs:
- mixed: bfloat16 [32, 4096], P(None, 'kv')
- log_weight: float32 [32, 32], P(None, 'tp')
Inputs may be any that keep to these rules, and one draw needn't show every extreme that they name: Columns of tokens come in 16 groups of equal width. `cum_gates`: each row does not rise along the positions. `lengths`: some sequence has all 10240 positions cached.
All inputs are finite; a program needn't handle non-finite values.
Results may differ from a plain program's by a relative error of at most 0.0307.
Values may be sent and summed in bfloat16 or wider, within the bound.
A program may use at most 128 MiB of HBM per device.

v0:
```python
import jax
import jax.numpy as jnp
from jax import lax
from jax.sharding import PartitionSpec as P

norm_eps = 1e-05
masked_floor = -1e30


def finish_rows(row_squares, sum_query, sum_keyval, sum_gate, forget_bias, model_width):
    row_scale = lax.rsqrt(row_squares / model_width + norm_eps)[:, None]
    query = (row_scale * sum_query).astype(jnp.bfloat16)
    keyval = (row_scale * sum_keyval).astype(jnp.bfloat16)
    log_gate = jax.nn.log_sigmoid(row_scale * sum_gate + forget_bias)
    return (query, keyval, log_gate)


def shards(
    tokens,
    norm_gain,
    w_query,
    w_key,
    w_value,
    forget_weight,
    forget_bias,
    kv_cache,
    cum_gates,
    lengths,
    w_out,
):
    rows_count, col_count = tokens.shape
    span_len = kv_cache.shape[1]
    kv_local = kv_cache.shape[2]
    head_size = kv_cache.shape[3] // 2
    heads_local = cum_gates.shape[1]
    group_size = heads_local // kv_local
    model_width = col_count * lax.axis_size("kv")
    tokens_f = tokens.astype(jnp.float32)
    squares = jnp.sum(tokens_f * tokens_f, axis=1)
    normalized_input = (tokens_f * norm_gain).astype(jnp.bfloat16)
    gate_cols = lax.dynamic_slice(
        forget_weight,
        (lax.axis_index("kv") * col_count, lax.axis_index("tp") * heads_local),
        (col_count, heads_local),
    )
    part_query = jnp.dot(normalized_input, w_query, preferred_element_type=jnp.float32)
    part_keyval = jnp.concatenate(
        [
            jnp.dot(normalized_input, w_key, preferred_element_type=jnp.float32),
            jnp.dot(normalized_input, w_value, preferred_element_type=jnp.float32),
        ],
        axis=1,
    )
    part_gate = jnp.dot(normalized_input, gate_cols, preferred_element_type=jnp.float32)
    total_sq, sum_query, sum_keyval, sum_gate = (
        lax.psum(squares.astype(jnp.bfloat16), "kv").astype(jnp.float32),
        lax.psum(part_query.astype(jnp.bfloat16), "kv").astype(jnp.float32),
        lax.psum(part_keyval.astype(jnp.bfloat16), "kv").astype(jnp.float32),
        lax.psum(part_gate.astype(jnp.bfloat16), "kv").astype(jnp.float32),
    )
    query, keyval, log_gate = finish_rows(
        total_sq, sum_query, sum_keyval, sum_gate, forget_bias, model_width
    )
    inv_root = head_size ** (-0.5)
    query_head_rows = query.reshape(rows_count, kv_local, group_size, head_size)
    cached_keys = kv_cache[:, :, :, :head_size]
    cached_vals = kv_cache[:, :, :, head_size:]
    scores = (
        jnp.einsum(
            "bkgd,blkd->bkgl", query_head_rows, cached_keys, preferred_element_type=jnp.float32
        )
        * inv_root
    )
    biased = scores - cum_gates.reshape(rows_count, kv_local, group_size, span_len)
    first_pos = lax.axis_index("kv") * span_len
    positions = first_pos + lax.iota(jnp.int32, span_len)
    in_range = positions[None, :] < lengths[:, None]
    last_pos = lengths - 1
    holds_last = (last_pos >= first_pos) & (last_pos < first_pos + span_len)
    last_index = jnp.clip(last_pos - first_pos, 0, span_len - 1)
    last_cum = jnp.take_along_axis(
        cum_gates, jnp.broadcast_to(last_index[:, None, None], (rows_count, heads_local, 1)), axis=2
    )[:, :, 0]
    cum_query = last_cum + log_gate
    fresh_key_row = keyval[:, : kv_local * head_size].reshape(rows_count, kv_local, head_size)
    value_new = keyval[:, kv_local * head_size :].reshape(rows_count, kv_local, head_size)
    new_biased = (
        jnp.einsum(
            "pnof,pnf->pno", query_head_rows, fresh_key_row, preferred_element_type=jnp.float32
        )
        * inv_root
    )
    new_biased = new_biased - cum_query.reshape(rows_count, kv_local, group_size)
    range_mask = in_range[:, None, None, :]
    owner_mask = holds_last[:, None, None]
    peak_local = jnp.max(jnp.where(range_mask, biased, masked_floor), axis=-1)
    peak_local = jnp.where(owner_mask, jnp.maximum(peak_local, new_biased), peak_local)
    weights = jnp.where(range_mask, jnp.exp(biased - peak_local[..., None]), 0.0)
    new_weight = jnp.where(owner_mask, jnp.exp(new_biased - peak_local), 0.0)
    weight_sum = jnp.sum(weights, axis=-1) + new_weight
    weighted = jnp.einsum(
        "bkgl,blkd->bkgd",
        weights.astype(jnp.bfloat16),
        cached_vals,
        preferred_element_type=jnp.float32,
    )
    weighted = (
        weighted
        + new_weight.astype(jnp.bfloat16).astype(jnp.float32)[..., None]
        * value_new.astype(jnp.float32)[:, :, None, :]
    )
    anchor = jnp.where(holds_last[:, None], cum_query, 0.0).reshape(
        rows_count, kv_local, group_size
    )
    peak = lax.pmax(peak_local, "kv")
    rescale_factor = jnp.exp(peak_local - peak)
    weight_sum, weighted, anchor = lax.psum(
        (weight_sum * rescale_factor, weighted * rescale_factor[..., None], anchor), "kv"
    )
    attended = (
        (weighted / weight_sum[..., None])
        .astype(jnp.bfloat16)
        .reshape(rows_count, heads_local * head_size)
    )
    log_weight = (peak + jnp.log(weight_sum) + anchor).reshape(rows_count, heads_local)
    part_out = jnp.dot(attended, w_out, preferred_element_type=jnp.float32)
    mixed = lax.psum(part_out.astype(jnp.bfloat16), "tp")
    return (mixed, log_weight)


def solution(mesh):
    placed = (
        P(None, "kv"),
        P("kv"),
        P("kv", "tp"),
        P("kv", "tp"),
        P("kv", "tp"),
        P(),
        P("tp"),
        P(None, "kv", "tp", None),
        P(None, "tp", "kv"),
        P(),
        P("tp", "kv"),
    )
    return jax.shard_map(
        shards,
        mesh=mesh,
        in_specs=placed,
        out_specs=(P(None, "kv"), P(None, "tp")),
        check_vma=False,
    )
```

profile of v0, /device:TPU:0, one launch (start us, length us, event | category | flops | bytes accessed | tf_op | source)
XLA Modules:
  0.0 224.6 jit_solution(18268263765218162662)
XLA Ops:
  7.3 41.6 %fusion.40 = (bf16[32,1280,2,64]{3,2,1,0:T(2,128)(2,1)}, bf16[32,1280,2,64]{3,2,1,0:T(2,128)(2,1)}) fusion(bf16[32,1280,2,128]{3,2,1,0:T(2,128)(2,1)} %param.18), kind=kLoop, calls=%fused_computation.64 | loop fusion | bytes 41943040 | tf_op jit(solution)/shard_map/slice | solution.py:66
  48.9 1.5 reshape.198
  50.4 0.1 fusion.22
  50.5 0.2 convolution_convert_fusion.1
  50.7 0.1 convolution_convert_fusion.2
  50.9 0.1 convolution_convert_fusion.3
  51.0 0.8 convolution_convert_fusion.4
  51.8 39.3 %all-reduce.1 = (bf16[32,512]{1,0:T(8,128)(2,1)S(1)}, bf16[32]{0:T(256)(128)(2,1)S(1)}, bf16[32,8]{0,1:T(8,128)(2,1)S(1)}, bf16[32,256]{1,0:T(8,128)(2,1)S(1)}) all-reduce(bf16[32,512]{1,0:T(8,128)(2,1)S(1)} %convolution_convert_fusion.1, bf16[32]{0:T(256)(128)(2,1)S(1)} %fusion.22, ...), channel_id=1, replica_groups=mesh['kv'=8,'tp'=4] {'kv'}, use_global_device_ids=true, to_apply=%region_2.0 | all-reduce | flops 24864 | bytes 99456 | tf_op jit(solution)/shard_map/psum | solution.py:57
  91.3 0.1 reshape.197
  91.4 0.1 broadcast_compare_fusion
  91.5 12.1 %select_reduce_fusion = (f32[32,2,4]{2,1,0:T(2,128)S(1)}, f32[32,2,4,1280]{3,2,1,0:T(4,128)S(1)}) fusion(pred[32,1280]{1,0:T(8,128)(4,1)S(1)} %broadcast_compare_fusion, f32[32,2,4,1280]{3,2,1,0:T(4,128)} %reshape.198, bf16[32,2,4,64]{3,2,1,0:T(4,128)(2,1)S(1)} %reshape.197, bf16[32,1280,2,64]{3,2,1,0:T(2,128)(2,1)} %get-tuple-element.15), kind=kOutput, calls=%fused_computation.8 | convolution fusion | flops 43253504 | bytes 13181952 | tf_op jit(solution)/shard_map/bkgd,blkd->bkgl/dot_general | solution.py:69
  103.6 0.1 copy.42
  103.9 0.1 reshape.207
  104.0 2.3 %gather_fusion = f32[256]{0:T(256)S(1)} fusion(f32[32,8,1280]{2,1,0:T(8,128)S(1)} %copy-done.2, s32[256]{0:T(256)S(1)} %reshape.207), kind=kCustom, calls=%fused_computation | custom fusion | bytes 5120 | tf_op jit(solution)/shard_map/jit(take_along_axis)/gather | solution.py:81
  106.6 0.2 fusion.41
  106.8 0.1 copy.51
  106.9 0.1 broadcast_select_fusion
  107.0 0.1 copy.44
  107.1 17.1 %pmax.7 = f32[32,2,4]{0,2,1:T(4,128)S(1)} all-reduce(f32[32,2,4]{0,2,1:T(4,128)S(1)} %maximum_select_fusion), channel_id=1, replica_groups=mesh['kv'=8,'tp'=4] {'kv'}, use_global_device_ids=true, to_apply=%region_6.7 | all-reduce | flops 256 | bytes 2048 | tf_op jit(solution)/shard_map/pmax | solution.py:115
  124.2 0.8 fusion.16
  125.0 0.1 copy.48
  125.1 0.1 copy.47
  125.3 0.1 copy.46
  125.4 10.7 %fusion.13 = f32[32,2,4,64]{3,2,1,0:T(4,128)} fusion(bf16[32,1280,2,64]{3,2,1,0:T(2,128)(2,1)} %get-tuple-element.16, f32[32,2,4,1280]{3,2,1,0:T(4,128)S(1)} %get-tuple-element.21, f32[32,2,4]{2,1,0:T(2,128)S(1)} %copy.44, pred[32,1280]{1,0:T(8,128)(4,1)S(1)} %broadcast_compare_fusion, f32[32,2,4]{2,1,0:T(2,128)S(1)} %copy.47, ...), kind=kOutput, calls=%fused_computation.10 | convolution fusion | flops 42975232 | bytes 11922432 | tf_op jit(solution)/shard_map/bkgl,blkd->bkgd/dot_general | solution.py:101
  136.2 19.6 %all-reduce = (f32[32,2,4]{0,2,1:T(4,128)S(1)}, f32[32,2,4]{0,2,1:T(4,128)S(1)}) all-reduce(f32[32,2,4]{0,2,1:T(4,128)S(1)} %get-tuple-element.10, f32[32,2,4]{0,2,1:T(4,128)S(1)} %bitcast.31), channel_id=1, replica_groups=mesh['kv'=8,'tp'=4] {'kv'}, use_global_device_ids=true, to_apply=%region_9.10 | all-reduce | flops 512 | bytes 4096 | tf_op jit(solution)/shard_map/psum | solution.py:117
  155.8 0.6 add_add_fusion
  156.4 0.1 copy.49
  156.5 49.0 %all-reduce.4.cloned.1.call-done = f32[32,2,4,64]{3,2,1,0:T(4,128)} async-done(((f32[32,2,4,64]{3,2,1,0:T(4,128)}), f32[32,2,4,64]{3,2,1,0:T(4,128)}) %all-reduce.4.cloned.1.call-update) | async-done | bytes 65552 | tf_op jit(solution)/shard_map/psum | solution.py:117
  205.5 1.0 divide_convert_fusion
  206.5 0.1 reshape.201
  206.7 0.2 convolution_convert_fusion
  206.9 10.9 %psum.62 = bf16[32,512]{1,0:T(8,128)(2,1)} all-reduce(bf16[32,512]{1,0:T(8,128)(2,1)S(1)} %convolution_convert_fusion), channel_id=1, replica_groups=mesh['kv'=8,'tp'=4] {'tp'}, use_global_device_ids=true, to_apply=%region_10.11 | all-reduce | flops 16384 | bytes 65536 | tf_op jit(solution)/shard_map/psum | solution.py:127
  (42 shorter events, 0.8 us)
Async XLA Ops:
  7.2 43.3 %copy-start = (bf16[512,512]{1,0:T(8,128)(2,1)S(1)}, bf16[512,512]{1,0:T(8,128)(2,1)}, u32[]{:S(2)}) copy-start(bf16[512,512]{1,0:T(8,128)(2,1)} %param.13) | copy-start | bytes 1572868
  7.2 198.3 %all-reduce.4.cloned.1.call-start = ((), (), s32[]{:S(2)}) async-start(), calls=%async_computation | async-start | bytes 262144 | tf_op jit(solution)/shard_map/psum | solution.py:117
  7.2 41.6 %copy-start.2 = (f32[32,8,1280]{2,1,0:T(8,128)S(1)}, f32[32,8,1280]{2,1,0:T(8,128)}, u32[]{:S(2)}) copy-start(f32[32,8,1280]{2,1,0:T(8,128)} %param.19) | copy-start | bytes 3932164
  48.9 1.5 copy-start.3
  48.9 1.6 copy-start.7
  48.9 1.8 copy-start.5
  48.9 2.0 copy-start.6
  48.9 42.5 %copy-start.8 = (s32[32]{0:T(128)S(1)}, s32[32]{0:T(128)}, u32[]{:S(2)}) copy-start(s32[32]{0:T(128)} %param.20) | copy-start | bytes 388
  103.9 2.9 %copy-start.9 = (f32[8]{0:T(128)S(1)}, f32[8]{0:T(128)}, u32[]{:S(2)}) copy-start(f32[8]{0:T(128)} %param.17) | copy-start | bytes 100
  125.4 81.3 %copy-start.4 = (bf16[512,512]{1,0:T(8,128)(2,1)S(1)}, bf16[512,512]{1,0:T(8,128)(2,1)}, u32[]{:S(2)}) copy-start(bf16[512,512]{1,0:T(8,128)(2,1)} %param.21) | copy-start | bytes 1572868
  125.4 92.3 %copy-start.1 = (bf16[512,512]{1,0:T(8,128)(2,1)S(1)}, bf16[512,512]{1,0:T(8,128)(2,1)}, u32[]{:S(2)}) copy-start(bf16[512,512]{1,0:T(8,128)(2,1)} %param.13) | copy-start | bytes 1572868
Sparse Core Ops, SparseCore 0:
  136.3 69.1 all-reduce.3
where the time goes:
time: 225 us
  blocking collectives  86.9 us (39%)
  waiting for transfers between devices  49 us (22%)
  local copies, waits for them, and re-layouts  46.8 us (21%)
  matrix products  24.5 us (11%)
  between operations  14.3 us (6%)
  other arithmetic  2.95 us (1%)
    psum x1, waiting for transfers between devices, shards(): lax.psum((weight_sum * rescale_factor, weighted * rescale_factor[..., Non...  49 us
    slice x1, local copies, waits for them, and re-layouts, shards(): cached_keys = kv_cache[:, :, :, :head_size]  41.6 us
    psum x1, blocking collectives, shards(): lax.psum(part_query.astype(jnp.bfloat16), 'kv').astype(jnp.float32)  39.3 us
    psum x1, blocking collectives, shards(): lax.psum((weight_sum * rescale_factor, weighted * rescale_factor[..., Non...  19.6 us
    pmax x1, blocking collectives, shards(): peak = lax.pmax(peak_local, 'kv')  17.1 us
    dot_general x1, matrix products, shards(): jnp.einsum('bkgd,blkd->bkgl', query_head_rows, cached_keys, preferred_ele...  12.1 us
    psum x1, blocking collectives, shards(): mixed = lax.psum(part_out.astype(jnp.bfloat16), 'tp')  10.9 us
    dot_general x1, matrix products, shards(): jnp.einsum('bkgl,blkd->bkgd', weights.astype(jnp.bfloat16), cached_vals,...  10.7 us
  transfers between devices with their start and end apart: 1, of which 1 were waited for; matrix products, arithmetic and copies ran while one was open for 0% of the time, Pallas kernels for 0%

commit v1 on v0

v1 whole, which is shorter than its diff:
```python
import functools
import jax
import jax.numpy as jnp
from jax import lax
from jax.experimental import pallas as pl
from jax.experimental.pallas import tpu as pltpu
from jax.sharding import PartitionSpec as P

norm_eps = 1e-05
masked_floor = -1e30
LANES = 128
MESH = pl.DeviceIdType.MESH


def flip(index, step, count):
    out = index
    bit = 1
    while bit < count:
        out = out + bit * ((step // bit) % 2) * (1 - 2 * ((index // bit) % 2))
        bit *= 2
    return out


def lane_of(shape):
    return lax.broadcasted_iota(jnp.int32, shape, len(shape) - 1)


def kernel(
    n_kv,
    n_tp,
    tokens_ref,
    gain_ref,
    bias_ref,
    lengths_ref,
    w_query_hbm,
    w_key_hbm,
    w_value_hbm,
    gate_hbm,
    cache_hbm,
    cum_hbm,
    w_out_hbm,
    mixed_ref,
    log_ref,
    w_query_ref,
    w_key_ref,
    w_value_ref,
    gate_ref,
    cache_ref,
    cum_ref,
    w_out_ref,
    shift_ref,
    last_ref,
    proj_ref,
    rs1_ref,
    query_ref,
    wide_ref,
    own_query_ref,
    own_key_ref,
    own_value_ref,
    own_gate_ref,
    part_ref,
    rs2_ref,
    comb_ref,
    att_ref,
    rows_ref,
    tp_ref,
    weight_sems,
    cache_sems,
    rs1_send,
    rs1_recv,
    ag1_send,
    ag1_recv,
    rs2_send,
    rs2_recv,
    ag2_send,
    ag2_recv,
    tp_send,
    tp_recv,
):
    f32, bf16 = jnp.float32, jnp.bfloat16
    me = lax.axis_index("kv")
    my_tp = lax.axis_index("tp")
    rows, cols = tokens_ref.shape
    heads = cum_ref.shape[1]
    span = cum_ref.shape[2]
    kv_local = cache_ref.shape[1] // span
    group = heads // kv_local
    head_size = LANES // 2
    all_heads = gate_hbm.shape[0]
    mine = rows // n_kv
    q_cols = w_query_ref.shape[1]
    k_cols = w_key_ref.shape[1]
    k_pad = -(-k_cols // LANES) * LANES
    model_width = cols * n_kv
    inv_root = head_size ** (-0.5)

    gate_ref[...] = jnp.zeros_like(gate_ref)
    offset = pl.multiple_of(me * cols, cols)
    loads = [
        pltpu.make_async_copy(src, dst, weight_sems.at[i])
        for i, (src, dst) in enumerate(
            [
                (w_query_hbm, w_query_ref),
                (w_key_hbm, w_key_ref),
                (w_value_hbm, w_value_ref),
                (gate_hbm.at[:, pl.ds(offset, cols)], gate_ref.at[pl.ds(0, all_heads)]),
                (cum_hbm, cum_ref),
                (w_out_hbm, w_out_ref),
            ]
        )
    ]
    for load in loads[:5]:
        load.start()

    def cache_load(owner):
        at = pl.ds(owner * mine, mine)
        return pltpu.make_async_copy(cache_hbm.at[at], cache_ref.at[at], cache_sems.at[owner])

    for step in range(n_kv):
        cache_load(flip(me, step, n_kv)).start()
    loads[5].start()

    barrier = pltpu.get_barrier_semaphore()
    for step in range(1, n_kv):
        pl.semaphore_signal(
            barrier, inc=1, device_id={"kv": flip(me, step, n_kv)}, device_id_type=MESH
        )
    for step in range(1, n_tp):
        pl.semaphore_signal(
            barrier, inc=1, device_id={"tp": flip(my_tp, step, n_tp)}, device_id_type=MESH
        )

    tokens_f = tokens_ref[...].astype(f32)
    squares = jnp.sum(tokens_f * tokens_f, axis=1, keepdims=True)
    normed = (tokens_f * gain_ref[...]).astype(bf16)
    for load in loads[:4]:
        load.wait()
    pieces = [jnp.dot(normed, w_query_ref[...], preferred_element_type=f32)]
    for w_ref in (w_key_ref, w_value_ref):
        piece = jnp.dot(normed, w_ref[...], preferred_element_type=f32)
        if k_pad > k_cols:
            piece = jnp.concatenate([piece, jnp.zeros((rows, k_pad - k_cols), f32)], axis=1)
        pieces.append(piece)
    gates = lax.dot_general(
        normed, gate_ref[...], (((1,), (1,)), ((), ())), preferred_element_type=f32
    )
    pieces.append(jnp.where(lane_of(gates.shape) == all_heads, squares, gates))
    at = 0
    for piece in pieces:
        for owner in range(n_kv):
            proj_ref[owner, :, at : at + piece.shape[1]] = piece[
                owner * mine : (owner + 1) * mine
            ].astype(bf16)
        at += piece.shape[1]

    pl.semaphore_wait(barrier, n_kv + n_tp - 2)

    def rs1_copy(source, target):
        return pltpu.make_async_remote_copy(
            src_ref=proj_ref.at[target],
            dst_ref=rs1_ref.at[source],
            send_sem=rs1_send.at[target],
            recv_sem=rs1_recv.at[source],
            device_id={"kv": target},
            device_id_type=MESH,
        )

    for step in reversed(range(1, n_kv)):
        rs1_copy(me, flip(me, step, n_kv)).start()

    loads[4].wait()
    tile = (heads, LANES)
    lane = lane_of(tile)
    own_column = (lane % kv_local) == (lax.broadcasted_iota(jnp.int32, tile, 0) // group)

    def prepare(row, carry):
        length = lengths_ref[row] - me * span
        last = jnp.zeros(tile, f32)
        for chunk in range(span // LANES):
            cum = cum_ref[row, :, chunk * LANES : (chunk + 1) * LANES]
            place = lane + chunk * LANES
            shift = jnp.where(place < length, -cum, masked_floor)
            last = last + jnp.where(place == length - 1, cum, 0.0)
            for part in range(kv_local):
                if kv_local == 1:
                    spread = shift
                else:
                    pick = lane // kv_local + part * (LANES // kv_local)
                    spread = jnp.take_along_axis(shift, pick, axis=1)
                    spread = jnp.where(own_column, spread, masked_floor)
                at = (chunk * kv_local + part) * LANES
                shift_ref[row, :, at : at + LANES] = spread
        last_ref[row] = jnp.broadcast_to(jnp.sum(last, axis=1, keepdims=True), tile)
        return carry

    lax.fori_loop(0, rows, prepare, 0, unroll=4)

    total = proj_ref[me].astype(f32)
    for step in range(1, n_kv):
        other = flip(me, step, n_kv)
        rs1_copy(other, me).wait_recv()
        total = total + rs1_ref[other].astype(f32)
    misc = total[:, q_cols + 2 * k_pad :]
    misc_lane = lane_of(misc.shape)
    total_sq = jnp.sum(jnp.where(misc_lane == all_heads, misc, 0.0), axis=1, keepdims=True)
    row_scale = lax.rsqrt(total_sq / model_width + norm_eps)
    query_ref[me] = (row_scale * total[:, :q_cols]).astype(bf16)

    def ag1_copy(source, target):
        return pltpu.make_async_remote_copy(
            src_ref=query_ref.at[source],
            dst_ref=query_ref.at[source],
            send_sem=ag1_send.at[target],
            recv_sem=ag1_recv.at[source],
            device_id={"kv": target},
            device_id_type=MESH,
        )

    for step in reversed(range(1, n_kv)):
        ag1_copy(me, flip(me, step, n_kv)).start()

    part_lane = lane_of((mine, LANES))

    def spread_heads(ref, values, which, upper):
        for head in range(heads):
            at = which(head)
            pair = values[:, (at // 2) * LANES : (at // 2 + 1) * LANES]
            if (at % 2 == 1) != upper:
                pair = pltpu.roll(pair, head_size, 1)
            keep = (part_lane >= head_size) if upper else (part_lane < head_size)
            ref[pl.ds(head, mine, stride=heads), :] = jnp.where(keep, pair, 0.0)

    new_kv = (row_scale * total[:, q_cols : q_cols + 2 * k_pad]).astype(bf16).astype(f32)
    spread_heads(own_query_ref, query_ref[me].astype(f32), lambda head: head, False)
    spread_heads(own_key_ref, new_kv[:, :k_pad], lambda head: head // group, False)
    spread_heads(own_value_ref, new_kv[:, k_pad:], lambda head: head // group, True)
    for head in range(heads):
        own_gate_ref[pl.ds(head, mine, stride=heads), :] = row_scale * misc

    def rs2_copy(source, target):
        return pltpu.make_async_remote_copy(
            src_ref=part_ref.at[target],
            dst_ref=rs2_ref.at[source],
            send_sem=rs2_send.at[target],
            recv_sem=rs2_recv.at[source],
            device_id={"kv": target},
            device_id_type=MESH,
        )

    length_cols = cache_ref.shape[1]
    chunk_cols = 2 * LANES
    zeros = jnp.zeros((heads, LANES), f32)

    def attend(step, carry):
        owner = flip(me, step, n_kv)

        @pl.when(step > 0)
        def _():
            ag1_copy(owner, me).wait_recv()

        cache_load(owner).wait()
        spread_heads(wide_ref, query_ref[owner].astype(f32) * inv_root, lambda head: head, False)
        for pair in range(mine // 2):
            first, second = 2 * pair, 2 * pair + 1
            row_a, row_b = owner * mine + first, owner * mine + second
            left = wide_ref[first * heads : (first + 1) * heads, :]
            right = wide_ref[second * heads : (second + 1) * heads, :]
            queries = jnp.concatenate(
                [
                    jnp.concatenate([left, zeros], axis=1),
                    jnp.concatenate([zeros, right], axis=1),
                ],
                axis=0,
            ).astype(bf16)

            def entries(at):
                return jnp.concatenate(
                    [cache_ref[row_a, at : at + chunk_cols, :], cache_ref[row_b, at : at + chunk_cols, :]],
                    axis=1,
                )

            biased = []
            peak = None
            for at in range(0, length_cols, chunk_cols):
                score = lax.dot_general(
                    queries, entries(at), (((1,), (1,)), ((), ())), preferred_element_type=f32
                )
                score = score + jnp.concatenate(
                    [shift_ref[row_a, :, at : at + chunk_cols], shift_ref[row_b, :, at : at + chunk_cols]],
                    axis=0,
                )
                biased.append(score)
                peak = score if peak is None else jnp.maximum(peak, score)
            peak = jnp.max(peak, axis=1, keepdims=True)
            sums = jnp.zeros((2 * heads, chunk_cols), f32)
            values = jnp.zeros((2 * heads, chunk_cols), f32)
            for i, at in enumerate(range(0, length_cols, chunk_cols)):
                weight = jnp.exp(biased[i] - peak)
                sums = sums + weight
                values = values + jnp.dot(
                    weight.astype(bf16), entries(at), preferred_element_type=f32
                )
            total_weight = jnp.sum(sums, axis=1, keepdims=True)
            for i, (place, row) in enumerate(((first, row_a), (second, row_b))):
                inside = slice(i * heads, (i + 1) * heads)
                out = values[inside, i * LANES : (i + 1) * LANES]
                out = jnp.where(lane == 0, peak[inside], out)
                out = jnp.where(lane == 1, total_weight[inside], out)
                out = jnp.where(lane == 2, last_ref[row], out)
                part_ref[owner, place * heads : (place + 1) * heads, :] = out

        @pl.when(step > 0)
        def _():
            rs2_copy(me, owner).start()

        return carry

    lax.fori_loop(0, n_kv, attend, 0)

    tall = (mine * heads, LANES)
    tall_lane = lane_of(tall)
    head_of = lax.broadcasted_iota(jnp.int32, tall, 0) % heads
    gate = jnp.sum(
        jnp.where(tall_lane == my_tp * heads + head_of, own_gate_ref[...], 0.0),
        axis=1,
        keepdims=True,
    )
    short = (mine * heads, heads)
    gate_bias = jnp.sum(
        jnp.where(
            lane_of(short) == lax.broadcasted_iota(jnp.int32, short, 0) % heads,
            jnp.broadcast_to(bias_ref[...], short),
            0.0,
        ),
        axis=1,
        keepdims=True,
    )
    gate = gate + gate_bias
    log_gate = jnp.minimum(gate, 0.0) - jnp.log1p(jnp.exp(-jnp.abs(gate)))
    new_score = (
        jnp.sum(own_query_ref[...] * own_key_ref[...], axis=1, keepdims=True) * inv_root
    )
    blocks = [part_ref[me]]
    for step in range(1, n_kv):
        other = flip(me, step, n_kv)
        rs2_copy(other, me).wait_recv()
        blocks.append(rs2_ref[other])
    last = blocks[0]
    for block in blocks[1:]:
        last = last + block
    cum_query = last[:, 2:3] + log_gate
    new_biased = new_score - cum_query
    peak = blocks[0]
    for block in blocks[1:]:
        peak = jnp.maximum(peak, block)
    peak = jnp.maximum(peak[:, 0:1], new_biased)
    new_weight = jnp.exp(new_biased - peak)
    values = new_weight.astype(bf16).astype(f32) * own_value_ref[...]
    for block in blocks:
        values = values + jnp.exp(block[:, 0:1] - peak) * block
    weight_sum = values[:, 1:2] + new_weight
    log_weight = peak + jnp.log(weight_sum) + cum_query
    comb_ref[...] = jnp.where(tall_lane < head_size, log_weight, values / weight_sum)

    tail = jnp.zeros((mine, LANES), f32)
    even = None
    for head in range(heads):
        row = comb_ref[pl.ds(head, mine, stride=heads), :]
        tail = jnp.where((part_lane == head) | (part_lane == heads + head), row, tail)
        if head % 2 == 0:
            even = pltpu.roll(row, head_size, 1)
        else:
            at = (head // 2) * LANES
            att_ref[me, :, at : at + LANES] = jnp.where(
                part_lane < head_size, even, row
            ).astype(bf16)
    coarse = tail.astype(bf16).astype(f32)
    att_ref[me, :, q_cols:] = jnp.where(part_lane < heads, coarse, tail - coarse).astype(bf16)

    def ag2_copy(source, target):
        return pltpu.make_async_remote_copy(
            src_ref=att_ref.at[source],
            dst_ref=att_ref.at[source],
            send_sem=ag2_send.at[target],
            recv_sem=ag2_recv.at[source],
            device_id={"kv": target},
            device_id_type=MESH,
        )

    for step in reversed(range(1, n_kv)):
        ag2_copy(me, flip(me, step, n_kv)).start()
    loads[5].wait()
    for step in range(1, n_kv):
        ag2_copy(flip(me, step, n_kv), me).wait_recv()
    for owner in range(n_kv):
        rows_ref[owner * mine : (owner + 1) * mine, :] = att_ref[owner].astype(f32)
    attended = rows_ref[:, :q_cols].astype(bf16)
    tp_ref[my_tp] = jnp.dot(attended, w_out_ref[...], preferred_element_type=f32).astype(bf16)

    def tp_copy(source, target):
        return pltpu.make_async_remote_copy(
            src_ref=tp_ref.at[source],
            dst_ref=tp_ref.at[source],
            send_sem=tp_send.at[target],
            recv_sem=tp_recv.at[source],
            device_id={"tp": target},
            device_id_type=MESH,
        )

    for step in reversed(range(1, n_tp)):
        tp_copy(my_tp, flip(my_tp, step, n_tp)).start()
    tails = rows_ref[:, q_cols:]
    log_ref[...] = tails[:, :heads] + tails[:, heads : 2 * heads]

    for step in range(1, n_kv):
        other = flip(me, step, n_kv)
        rs1_copy(me, other).wait_send()
        ag1_copy(me, other).wait_send()
        rs2_copy(me, other).wait_send()
        ag2_copy(me, other).wait_send()
    for step in range(1, n_tp):
        tp_copy(flip(my_tp, step, n_tp), my_tp).wait_recv()
    mixed = tp_ref[0].astype(f32)
    for source in range(1, n_tp):
        mixed = mixed + tp_ref[source].astype(f32)
    mixed_ref[...] = mixed.astype(bf16)
    for step in range(1, n_tp):
        tp_copy(my_tp, flip(my_tp, step, n_tp)).wait_send()


def shards(
    tokens,
    norm_gain,
    w_query,
    w_key,
    w_value,
    forget_weight,
    forget_bias,
    kv_cache,
    cum_gates,
    lengths,
    w_out,
):
    n_kv, n_tp = lax.axis_size("kv"), lax.axis_size("tp")
    rows, cols = tokens.shape
    span, kv_local, entry = kv_cache.shape[1:]
    heads = cum_gates.shape[1]
    q_cols, k_cols = w_query.shape[1], w_key.shape[1]
    k_pad = -(-k_cols // LANES) * LANES
    wide = q_cols + 2 * k_pad + LANES
    mine = rows // n_kv
    out_cols = w_out.shape[1]
    f32, bf16 = jnp.float32, jnp.bfloat16
    vmem = pl.BlockSpec(memory_space=pltpu.VMEM)
    smem = pl.BlockSpec(memory_space=pltpu.SMEM)
    hbm = pl.BlockSpec(memory_space=pl.ANY)
    dma = pltpu.SemaphoreType.DMA
    tall = (mine * heads, LANES)
    return pl.pallas_call(
        functools.partial(kernel, n_kv, n_tp),
        out_shape=(
            jax.ShapeDtypeStruct((rows, out_cols), bf16),
            jax.ShapeDtypeStruct((rows, heads), f32),
        ),
        in_specs=[vmem, vmem, vmem, smem] + [hbm] * 7,
        out_specs=(vmem, vmem),
        scratch_shapes=[
            pltpu.VMEM(w_query.shape, bf16),
            pltpu.VMEM(w_key.shape, bf16),
            pltpu.VMEM(w_value.shape, bf16),
            pltpu.VMEM((LANES, cols), bf16),
            pltpu.VMEM((rows, span * kv_local, entry), bf16),
            pltpu.VMEM(cum_gates.shape, f32),
            pltpu.VMEM(w_out.shape, bf16),
            pltpu.VMEM((rows, heads, span * kv_local), f32),
            pltpu.VMEM((rows, heads, LANES), f32),
            pltpu.VMEM((n_kv, mine, wide), bf16),
            pltpu.VMEM((n_kv, mine, wide), bf16),
            pltpu.VMEM((n_kv, mine, q_cols), bf16),
            pltpu.VMEM(tall, f32),
            pltpu.VMEM(tall, f32),
            pltpu.VMEM(tall, f32),
            pltpu.VMEM(tall, f32),
            pltpu.VMEM(tall, f32),
            pltpu.VMEM((n_kv,) + tall, f32),
            pltpu.VMEM((n_kv,) + tall, f32),
            pltpu.VMEM(tall, f32),
            pltpu.VMEM((n_kv, mine, q_cols + LANES), bf16),
            pltpu.VMEM((rows, q_cols + LANES), f32),
            pltpu.VMEM((n_tp, rows, out_cols), bf16),
            dma((6,)),
            dma((n_kv,)),
        ]
        + [dma((n_kv,))] * 8
        + [dma((n_tp,))] * 2,
        compiler_params=pltpu.CompilerParams(
            collective_id=0, has_side_effects=True, vmem_limit_bytes=56 * 1024 * 1024
        ),
    )(
        tokens,
        norm_gain.reshape(1, cols),
        forget_bias.reshape(1, heads),
        lengths,
        w_query,
        w_key,
        w_value,
        forget_weight.T,
        kv_cache.reshape(rows, span * kv_local, entry),
        cum_gates,
        w_out,
    )


def solution(mesh):
    placed = (
        P(None, "kv"),
        P("kv"),
        P("kv", "tp"),
        P("kv", "tp"),
        P("kv", "tp"),
        P(),
        P("tp"),
        P(None, "kv", "tp", None),
        P(None, "tp", "kv"),
        P(),
        P("tp", "kv"),
    )
    return jax.shard_map(
        shards,
        mesh=mesh,
        in_specs=placed,
        out_specs=(P(None, "kv"), P(None, "tp")),
        check_vma=False,
    )
```

time: 225 us -> 45.5 us (0.20)
  blocking collectives: 86.9 us -> 0 us
  waiting for transfers between devices: 49 us -> 0 us
  local copies, waits for them, and re-layouts: 46.8 us -> 2.75 us
  Pallas kernels: 0 us -> 41.8 us
  matrix products: 24.5 us -> 0 us
  between operations: 14.3 us -> 0.64 us
  other arithmetic: 2.95 us -> 0 us
    psum x3 -> x0, blocking collectives: 69.8 us -> none  [the longest x1 39.3 us: shards(): lax.psum(part_query.astype(jnp.bfloat16), 'kv').astype(jnp.float32)]
    psum x1 -> x0, waiting for transfers between devices: 49 us -> none  [shards(): lax.psum((weight_sum * rescale_factor, weighted * rescale_factor[..., Non...]
    pallas_call x0 -> x1, Pallas kernels: none -> 41.8 us  [shards(): pl.pallas_call(functools.partial(kernel, n_kv, n_tp), out_shape=(jax.Shap...]
    slice x1 -> x0, local copies, waits for them, and re-layouts: 41.6 us -> none  [shards(): cached_keys = kv_cache[:, :, :, :head_size]]
    dot_general x8 -> x0, matrix products: 24.5 us -> none  [the longest x1 12.1 us: shards(): jnp.einsum('bkgd,blkd->bkgl', query_head_rows, cached_keys, preferred_ele...]
    pmax x1 -> x0, blocking collectives: 17.1 us -> none  [shards(): peak = lax.pmax(peak_local, 'kv')]
    gather x5 -> x0, local copies, waits for them, and re-layouts: 2.58 us -> none  [shards(): jnp.take_along_axis(cum_gates, jnp.broadcast_to(last_index[:, None, None]...]
  transfers between devices with their start and end apart: 1 -> 0, of which waited for: 1 -> 0; matrix products, arithmetic and copies ran while one was open for 0% -> 0% of each run, Pallas kernels for 0% -> 0%
where the time goes in v1:
time: 45.5 us; the launch traced here: 45.2 us
  Pallas kernels  41.8 us (92%)
  local copies, waits for them, and re-layouts  2.75 us (6%)
  between operations  0.64 us (1%)
    pallas_call x1, Pallas kernels, shards(): pl.pallas_call(functools.partial(kernel, n_kv, n_tp), out_shape=(jax.Shap...  41.8 us
    pallas_call x1, local copies, waits for them, and re-layouts, shards(): pl.pallas_call(functools.partial(kernel, n_kv, n_tp), out_shape=(jax.Shap...  1.38 us
    unnamed x1, local copies, waits for them, and re-layouts  1.37 us

profile of v1, /device:TPU:0, one launch (start us, length us, event | category | flops | bytes accessed | tf_op | source)
XLA Modules:
  0.0 45.2 jit_solution(6934139429644141424)
XLA Ops:
  0.6 41.8 %shard_map.122 = (bf16[32,512]{1,0:T(8,128)(2,1)}, f32[32,8]{1,0:T(8,128)}) custom-call(bf16[32,512]{1,0:T(8,128)(2,1)} %tokens_ref.1, f32[1,512]{1,0:T(1,128)} %bitcast.6, f32[1,8]{1,0:T(1,128)} %bitcast.7, s32[32]{0:T(128)} %lengths_ref.1, bf16[512,512]{1,0:T(8,128)(2,1)} %w_query_hbm.1, bf16[512,128]{1,0:T(8,128)(2,1)} %w_key_hbm.1, ...), custom_call_target="tpu_custom_call" | custom-call | tf_op jit(solution)/shard_map/pallas_call | solution.py:459
  42.5 1.4 %copy.13 = f32[32,8]{0,1:T(8,128)} copy(f32[32,8]{1,0:T(8,128)} %get-tuple-element.3) | data formatting | bytes 2048 | tf_op jit(solution)/shard_map/pallas_call | solution.py:459
  43.8 1.4 %copy.15 = bf16[32,512]{1,0:T(8,128)(2,1)} copy(bf16[32,512]{1,0:T(8,128)(2,1)} %get-tuple-element.6) | data formatting | bytes 65536

commit v2 on v1

--- a/solution.py
+++ b/solution.py
@@ -54,6 +54,8 @@
     rs1_ref,
     query_ref,
     wide_ref,
+    score_ref,
+    peak_ref,
     own_query_ref,
     own_key_ref,
     own_value_ref,
@@ -116,10 +118,6 @@
         at = pl.ds(owner * mine, mine)
         return pltpu.make_async_copy(cache_hbm.at[at], cache_ref.at[at], cache_sems.at[owner])
 
-    for step in range(n_kv):
-        cache_load(flip(me, step, n_kv)).start()
-    loads[5].start()
-
     barrier = pltpu.get_barrier_semaphore()
     for step in range(1, n_kv):
         pl.semaphore_signal(
@@ -135,6 +133,9 @@
     normed = (tokens_f * gain_ref[...]).astype(bf16)
     for load in loads[:4]:
         load.wait()
+    for step in range(n_kv):
+        cache_load(flip(me, step, n_kv)).start()
+    loads[5].start()
     pieces = [jnp.dot(normed, w_query_ref[...], preferred_element_type=f32)]
     for w_ref in (w_key_ref, w_value_ref):
         piece = jnp.dot(normed, w_ref[...], preferred_element_type=f32)
@@ -249,65 +250,86 @@
 
     length_cols = cache_ref.shape[1]
     chunk_cols = 2 * LANES
+    chunks = range(0, length_cols, chunk_cols)
     zeros = jnp.zeros((heads, LANES), f32)
-
-    def attend(step, carry):
-        owner = flip(me, step, n_kv)
-
-        @pl.when(step > 0)
-        def _():
-            ag1_copy(owner, me).wait_recv()
-
+    pairs = range(mine // 2)
+
+    def entries(row_a, row_b, at):
+        inside = slice(at, at + chunk_cols)
+        return jnp.concatenate([cache_ref[row_a, inside, :], cache_ref[row_b, inside, :]], axis=1)
+
+    def weigh(pair):
+        peak = peak_ref[pair, :, :1]
+        sums = jnp.zeros((2 * heads, chunk_cols), f32)
+        weights = []
+        for at in chunks:
+            weight = jnp.exp(score_ref[pair, :, at : at + chunk_cols] - peak)
+            sums = sums + weight
+            weights.append(weight.astype(bf16))
+        return weights, jnp.sum(sums, axis=1, keepdims=True), peak
+
+    def score(owner, pair):
+        first, second = 2 * pair, 2 * pair + 1
+        row_a, row_b = owner * mine + first, owner * mine + second
+        left = wide_ref[first * heads : (first + 1) * heads, :]
+        right = wide_ref[second * heads : (second + 1) * heads, :]
+        queries = jnp.concatenate(
+            [
+                jnp.concatenate([left, zeros], axis=1),
+                jnp.concatenate([zeros, right], axis=1),
+            ],
+            axis=0,
+        ).astype(bf16)
+        peak = None
+        for at in chunks:
+            part = lax.dot_general(
+                queries,
+                entries(row_a, row_b, at),
+                (((1,), (1,)), ((), ())),
+                preferred_element_type=f32,
+            )
+            part = part + jnp.concatenate(
+                [shift_ref[row_a, :, at : at + chunk_cols], shift_ref[row_b, :, at : at + chunk_cols]],
+                axis=0,
+            )
+            score_ref[pair, :, at : at + chunk_cols] = part
+            peak = part if peak is None else jnp.maximum(peak, part)
+        peak_ref[pair] = jnp.broadcast_to(
+            jnp.max(peak, axis=1, keepdims=True), (2 * heads, LANES)
+        )
+
+    def gather(owner, pair, weights, total_weight, peak):
+        first, second = 2 * pair, 2 * pair + 1
+        row_a, row_b = owner * mine + first, owner * mine + second
+        values = jnp.zeros((2 * heads, chunk_cols), f32)
+        for weight, at in zip(weights, chunks):
+            values = values + jnp.dot(
+                weight, entries(row_a, row_b, at), preferred_element_type=f32
+            )
+        for i, (place, row) in enumerate(((first, row_a), (second, row_b))):
+            inside = slice(i * heads, (i + 1) * heads)
+            out = values[inside, i * LANES : (i + 1) * LANES]
+            out = jnp.where(lane == 0, peak[inside], out)
+            out = jnp.where(lane == 1, total_weight[inside], out)
+            out = jnp.where(lane == 2, last_ref[row], out)
+            part_ref[owner, place * heads : (place + 1) * heads, :] = out
+
+    def ready(owner):
         cache_load(owner).wait()
         spread_heads(wide_ref, query_ref[owner].astype(f32) * inv_root, lambda head: head, False)
-        for pair in range(mine // 2):
-            first, second = 2 * pair, 2 * pair + 1
-            row_a, row_b = owner * mine + first, owner * mine + second
-            left = wide_ref[first * heads : (first + 1) * heads, :]
-            right = wide_ref[second * heads : (second + 1) * heads, :]
-            queries = jnp.concatenate(
-                [
-                    jnp.concatenate([left, zeros], axis=1),
-                    jnp.concatenate([zeros, right], axis=1),
-                ],
-                axis=0,
-            ).astype(bf16)
-
-            def entries(at):
-                return jnp.concatenate(
-                    [cache_ref[row_a, at : at + chunk_cols, :], cache_ref[row_b, at : at + chunk_cols, :]],
-                    axis=1,
-                )
-
-            biased = []
-            peak = None
-            for at in range(0, length_cols, chunk_cols):
-                score = lax.dot_general(
-                    queries, entries(at), (((1,), (1,)), ((), ())), preferred_element_type=f32
-                )
-                score = score + jnp.concatenate(
-                    [shift_ref[row_a, :, at : at + chunk_cols], shift_ref[row_b, :, at : at + chunk_cols]],
-                    axis=0,
-                )
-                biased.append(score)
-                peak = score if peak is None else jnp.maximum(peak, score)
-            peak = jnp.max(peak, axis=1, keepdims=True)
-            sums = jnp.zeros((2 * heads, chunk_cols), f32)
-            values = jnp.zeros((2 * heads, chunk_cols), f32)
-            for i, at in enumerate(range(0, length_cols, chunk_cols)):
-                weight = jnp.exp(biased[i] - peak)
-                sums = sums + weight
-                values = values + jnp.dot(
-                    weight.astype(bf16), entries(at), preferred_element_type=f32
-                )
-            total_weight = jnp.sum(sums, axis=1, keepdims=True)
-            for i, (place, row) in enumerate(((first, row_a), (second, row_b))):
-                inside = slice(i * heads, (i + 1) * heads)
-                out = values[inside, i * LANES : (i + 1) * LANES]
-                out = jnp.where(lane == 0, peak[inside], out)
-                out = jnp.where(lane == 1, total_weight[inside], out)
-                out = jnp.where(lane == 2, last_ref[row], out)
-                part_ref[owner, place * heads : (place + 1) * heads, :] = out
+
+    ready(me)
+    for pair in pairs:
+        score(me, pair)
+
+    def attend(step, carry):
+        owner, after = flip(me, step, n_kv), flip(me, step + 1, n_kv)
+        ag1_copy(after, me).wait_recv()
+        ready(after)
+        for pair in pairs:
+            weights = weigh(pair)
+            score(after, pair)
+            gather(owner, pair, *weights)
 
         @pl.when(step > 0)
         def _():
@@ -315,7 +337,11 @@
 
         return carry
 
-    lax.fori_loop(0, n_kv, attend, 0)
+    lax.fori_loop(0, n_kv - 1, attend, 0)
+    final = flip(me, n_kv - 1, n_kv)
+    for pair in pairs:
+        gather(final, pair, *weigh(pair))
+    rs2_copy(me, final).start()
 
     tall = (mine * heads, LANES)
     tall_lane = lane_of(tall)
@@ -478,6 +504,8 @@
             pltpu.VMEM((n_kv, mine, wide), bf16),
             pltpu.VMEM((n_kv, mine, q_cols), bf16),
             pltpu.VMEM(tall, f32),
+            pltpu.VMEM((mine // 2, 2 * heads, span * kv_local), f32),
+            pltpu.VMEM((mine // 2, 2 * heads, LANES), f32),
             pltpu.VMEM(tall, f32),
             pltpu.VMEM(tall, f32),
             pltpu.VMEM(tall, f32),

time: 45.5 us -> 39.3 us (0.86)
  Pallas kernels: 41.8 us -> 35.6 us
    pallas_call x1, Pallas kernels: 41.8 us -> 35.6 us  [shards(): pl.pallas_call(functools.partial(kernel, n_kv, n_tp), out_shape=(jax.Shap...]
where the time goes in v2:
time: 39.3 us; the launch traced here: 39 us
  Pallas kernels  35.6 us (91%)
  local copies, waits for them, and re-layouts  2.75 us (7%)
  between operations  0.64 us (2%)
    pallas_call x1, Pallas kernels, shards(): pl.pallas_call(functools.partial(kernel, n_kv, n_tp), out_shape=(jax.Shap...  35.6 us
    pallas_call x1, local copies, waits for them, and re-layouts, shards(): pl.pallas_call(functools.partial(kernel, n_kv, n_tp), out_shape=(jax.Shap...  1.38 us
    unnamed x1, local copies, waits for them, and re-layouts  1.37 us

profile of v2, /device:TPU:0, one launch (start us, length us, event | category | flops | bytes accessed | tf_op | source)
XLA Modules:
  0.0 39.0 jit_solution(11912917027176285694)
XLA Ops:
  0.6 35.6 %shard_map.122 = (bf16[32,512]{1,0:T(8,128)(2,1)}, f32[32,8]{1,0:T(8,128)}) custom-call(bf16[32,512]{1,0:T(8,128)(2,1)} %tokens_ref.1, f32[1,512]{1,0:T(1,128)} %bitcast.6, f32[1,8]{1,0:T(1,128)} %bitcast.7, s32[32]{0:T(128)} %lengths_ref.1, bf16[512,512]{1,0:T(8,128)(2,1)} %w_query_hbm.1, bf16[512,128]{1,0:T(8,128)(2,1)} %w_key_hbm.1, ...), custom_call_target="tpu_custom_call" | custom-call | tf_op jit(solution)/shard_map/pallas_call | solution.py:485
  36.2 1.4 %copy.13 = f32[32,8]{0,1:T(8,128)} copy(f32[32,8]{1,0:T(8,128)} %get-tuple-element.3) | data formatting | bytes 2048 | tf_op jit(solution)/shard_map/pallas_call | solution.py:485
  37.6 1.4 %copy.15 = bf16[32,512]{1,0:T(8,128)(2,1)} copy(bf16[32,512]{1,0:T(8,128)(2,1)} %get-tuple-element.6) | data formatting | bytes 65536
